TPU v7x, 32 devices: a whole 2x2x4 slice. The times are simulated.
32 devices in a mesh: rep: 2 (over y), fs: 4 (over z), tp: 4 (over x, core).
Axes of the slice: x: 2, y: 2, z: 4, core: 2. Of those that a mesh axis runs over, the one named last changes fastest.
Arguments:
- tokens: bfloat16 [4096, 2048], P(('rep', 'fs'), 'tp'), may hold values from -6 to 6
- outer_gate: float32 [2048, 512], P('fs', 'tp'), may hold values from -0.125 to 0.125
- inner_gate: float32 [2048, 512], P('fs', 'tp'), may hold values from -0.125 to 0.125
- mixer_value: float32 [2048, 512], P('fs', 'tp'), may hold values from -0.125 to 0.125
- mixer_scales: float32 [3, 512], P(None, 'tp'), may hold values from 0.5 to 2
- mixer_taps: float32 [3, 512], P(None, 'tp'), may hold values from -3.5 to 3.5
- mixer_out: float32 [512, 2048], P('fs', 'tp'), may hold values from -0.25 to 0.25
- out_scale: float32 [2048], P('tp'), may hold values from 0.3 to 3
- first_gain: float32 [2048], replicated, may hold values from 0.1 to 1.9
- first_shift: float32 [2048], replicated, may hold values from -2 to 2
- up_proj: float32 [2048, 3072], P('fs', 'tp'), may hold values from -0.125 to 0.125
- gate_proj: float32 [2048, 3072], P('fs', 'tp'), may hold values from -0.125 to 0.125
- up_scales: float32 [2, 3072], P(None, 'tp'), may hold values from 0.5 to 2
- ffn_taps: float32 [3, 2, 3072], P(None, None, 'tp'), may hold values from -3.5 to 3.5
- ffn_shift: float32 [2, 3072], P(None, 'tp'), may hold values from -3 to 3
- down_proj: float32 [3072, 2048], P('fs', 'tp'), may hold values from -0.109375 to 0.109375
- down_scale: float32 [2048], P('tp'), may hold values from 0.3 to 3
- second_gain: float32 [2048], replicated, may hold values from 0.1 to 1.9
- second_shift: float32 [2048], replicated, may hold values from -2 to 2
Outputs:
- layer_out: bfloat16 [4096, 2048], P(('rep', 'fs'), 'tp')
All inputs are finite; a program needn't handle non-finite values.
Results may differ from a plain program's by a relative error of at most 0.017.
Values may be sent and summed in bfloat16 or wider, within the bound.
A program may use at most 64 MiB of HBM per device.

v0:
```python
import jax
import jax.numpy as jnp
from jax import lax
from jax.sharding import PartitionSpec as P

LEN = 128
norm_eps = 1e-05
residual_weight = 8.0**0.25


def causal_mix(signal, kernel_taps):
    sequences = signal.reshape(-1, LEN, signal.shape[-1])
    padded = jnp.pad(sequences, ((0, 0), (2, 0), (0, 0)))
    mixed = (
        kernel_taps[0] * padded[:, :-2]
        + kernel_taps[1] * padded[:, 1:-1]
        + kernel_taps[2] * padded[:, 2:]
    )
    return mixed.reshape(signal.shape)


def lowered(matrix):
    return matrix.astype(jnp.bfloat16)


def single_fold(operand, portion):
    return jnp.dot(operand, portion, preferred_element_type=jnp.float32)


def fold_step(operand, pieces):
    result = []
    for number in range(len(pieces)):
        result.append(jnp.dot(operand, pieces[number], preferred_element_type=jnp.float32))
    return tuple(result)


def own_columns(vector, own_width):
    return lax.dynamic_slice_in_dim(vector, lax.axis_index("tp") * own_width, own_width, 0)


def scaled_norm(summed, average, spread, gain_vector, shift_vector):
    return (summed - average) * lax.rsqrt(spread + norm_eps) * gain_vector + shift_vector


def local(
    tokens,
    outer_gate,
    inner_gate,
    mixer_value,
    mixer_scales,
    mixer_taps,
    mixer_out,
    out_scale,
    first_gain,
    first_shift,
    up_proj,
    gate_proj,
    up_scales,
    ffn_taps,
    ffn_shift,
    down_proj,
    down_scale,
    second_gain,
    second_shift,
):
    own_width = tokens.shape[1]
    full_width = own_width * lax.axis_size("tp")
    token_whole = lax.all_gather(tokens, "tp", axis=1, tiled=True)
    outer_part, inner_part, value_part = fold_step(
        token_whole,
        (
            lax.all_gather(lowered(outer_gate), "fs", axis=0, tiled=True),
            lax.all_gather(lowered(inner_gate), "fs", axis=0, tiled=True),
            lax.all_gather(lowered(mixer_value), "fs", axis=0, tiled=True),
        ),
    )
    outer_part = (outer_part * mixer_scales[0]).astype(jnp.bfloat16)
    inner_part = (inner_part * mixer_scales[1]).astype(jnp.bfloat16)
    value_part = (value_part * mixer_scales[2]).astype(jnp.bfloat16)
    product = inner_part.astype(jnp.float32) * value_part.astype(jnp.float32)
    mixed_conv = (outer_part.astype(jnp.float32) * causal_mix(product, mixer_taps)).astype(
        jnp.bfloat16
    )
    conv_whole = lax.all_gather(mixed_conv, "tp", axis=1, tiled=True)
    mixer_sum = (
        single_fold(conv_whole, lax.all_gather(lowered(mixer_out), "fs", axis=0, tiled=True))
        * out_scale
    )
    first_sum = residual_weight * tokens.astype(jnp.float32) + mixer_sum
    row_total, row_square = lax.psum(
        (jnp.sum(first_sum, 1, keepdims=True), jnp.sum(first_sum * first_sum, 1, keepdims=True)),
        "tp",
    )
    average = row_total / full_width
    spread = row_square / full_width - average * average
    normed = scaled_norm(
        first_sum,
        average,
        spread,
        own_columns(first_gain, own_width),
        own_columns(first_shift, own_width),
    ).astype(jnp.bfloat16)
    normed_whole = lax.all_gather(normed, "tp", axis=1, tiled=True)
    up_matrix, gate_matrix = (
        lax.all_gather(lowered(up_proj), "fs", axis=0, tiled=True),
        lax.all_gather(lowered(gate_proj), "fs", axis=0, tiled=True),
    )
    up_linear = jnp.dot(normed_whole, up_matrix, preferred_element_type=jnp.float32)
    gate_linear = jnp.dot(normed_whole, gate_matrix, preferred_element_type=jnp.float32)
    up_linear = up_linear * up_scales[0]
    gate_linear = gate_linear * up_scales[1]
    up_mixed = causal_mix(up_linear, ffn_taps[:, 0]) + ffn_shift[0]
    gate_mixed = causal_mix(gate_linear, ffn_taps[:, 1]) + ffn_shift[1]
    hidden = (up_mixed * jax.nn.silu(gate_mixed)).astype(jnp.bfloat16)
    hidden_whole = lax.all_gather(hidden, "tp", axis=1, tiled=True)
    ffn_sum = (
        single_fold(hidden_whole, lax.all_gather(lowered(down_proj), "fs", axis=0, tiled=True))
        * down_scale
    )
    second_sum = residual_weight * normed.astype(jnp.float32) + ffn_sum
    second_total, second_square = lax.psum(
        (jnp.sum(second_sum, 1, keepdims=True), jnp.sum(second_sum * second_sum, 1, keepdims=True)),
        "tp",
    )
    second_average = second_total / full_width
    second_spread = second_square / full_width - second_average * second_average
    return scaled_norm(
        second_sum,
        second_average,
        second_spread,
        own_columns(second_gain, own_width),
        own_columns(second_shift, own_width),
    ).astype(jnp.bfloat16)


def solution(mesh):
    return jax.shard_map(
        local,
        mesh=mesh,
        in_specs=(
            P(("rep", "fs"), "tp"),
            P("fs", "tp"),
            P("fs", "tp"),
            P("fs", "tp"),
            P(None, "tp"),
            P(None, "tp"),
            P("fs", "tp"),
            P("tp"),
            P(),
            P(),
            P("fs", "tp"),
            P("fs", "tp"),
            P(None, "tp"),
            P(None, None, "tp"),
            P(None, "tp"),
            P("fs", "tp"),
            P("tp"),
            P(),
            P(),
        ),
        out_specs=P(("rep", "fs"), "tp"),
        check_vma=False,
    )
```

profile of v0, /device:TPU:0, one launch (start us, length us, event | category | flops | bytes accessed | tf_op | source)
XLA Modules:
  0.0 314.0 jit_solution(7180715300881190758)
XLA Ops:
  6.5 0.0 all-gather.7.cloned.1.call-start
  6.5 0.7 all-gather.7.cloned.1.call-update
  7.3 0.0 copy-start.2
  7.3 0.0 copy-start.6
  7.3 0.0 all-gather.11.cloned.1.call-start
  7.3 2.4 convert_element_type.76
  9.8 0.0 all-gather.11.cloned.1.call-update
  9.8 0.0 all-gather.9.cloned.1.call-start
  9.9 1.0 copy.22
  11.0 0.0 copy-done.9
  11.0 0.0 copy-start.13
  11.0 0.0 copy-start.14
  11.0 0.8 dynamic_slice.12
  11.8 0.8 dynamic_slice.13
  12.5 17.4 %all_gather.36 = bf16[2048,128]{1,0:T(8,128)(2,1)S(1)} all-gather(bf16[512,128]{1,0:T(8,128)(2,1)S(1)} %convert_element_type.69), channel_id=1, replica_groups=mesh['rep'=2,'fs'=4,'tp'=4] {'fs'}, dimensions={0}, use_global_device_ids=true | all-gather | bytes 655360 | tf_op jit(solution)/shard_map/all_gather | solution.py:74
  29.9 16.9 %all_gather.35 = bf16[2048,128]{1,0:T(8,128)(2,1)S(1)} all-gather(bf16[512,128]{1,0:T(8,128)(2,1)S(1)} %convert_element_type.66), channel_id=1, replica_groups=mesh['rep'=2,'fs'=4,'tp'=4] {'fs'}, dimensions={0}, use_global_device_ids=true | all-gather | bytes 655360 | tf_op jit(solution)/shard_map/all_gather | solution.py:73
  46.8 22.6 %all_gather.34 = bf16[2048,128]{1,0:T(8,128)(2,1)S(1)} all-gather(bf16[512,128]{1,0:T(8,128)(2,1)S(1)} %convert_element_type.63), channel_id=1, replica_groups=mesh['rep'=2,'fs'=4,'tp'=4] {'fs'}, dimensions={0}, use_global_device_ids=true | all-gather | bytes 655360 | tf_op jit(solution)/shard_map/all_gather | solution.py:72
  69.4 20.2 %all_gather.38 = bf16[512,512]{1,0:T(8,128)(2,1)S(1)} all-gather(bf16[128,512]{1,0:T(8,128)(2,1)S(1)} %convert_element_type.73), channel_id=1, replica_groups=mesh['rep'=2,'fs'=4,'tp'=4] {'fs'}, dimensions={0}, use_global_device_ids=true | all-gather | bytes 655360 | tf_op jit(solution)/shard_map/all_gather | solution.py:86
  89.6 0.0 copy-done.13
  89.6 0.0 all-gather.7.cloned.1.call-done
  89.6 2.5 fusion.20
  92.1 0.7 fusion.18
  92.8 0.1 fusion.23
  92.9 0.0 copy-start.5
  92.9 0.0 copy-start.15
  92.9 0.7 fusion.15
  93.7 7.0 %all_gather.37 = bf16[512,512]{1,0:T(8,128)(2,1)S(1)} all-gather(bf16[512,128]{1,0:T(8,128)(2,1)S(1)} %fusion.15), channel_id=1, replica_groups=mesh['rep'=2,'fs'=4,'tp'=4] {'tp'}, dimensions={1}, use_global_device_ids=true | all-gather | bytes 655360 | tf_op jit(solution)/shard_map/all_gather | solution.py:84
  100.7 0.0 copy-done.15
  100.7 0.6 fusion.26
  101.3 0.0 copy-start.3
  101.3 7.0 %all-reduce.4 = (f32[512,1]{0,1:T(1,128)S(1)}, f32[512,1]{0,1:T(1,128)S(1)}) all-reduce(f32[512,1]{0,1:T(1,128)S(1)} %bitcast.57, f32[512,1]{0,1:T(1,128)S(1)} %bitcast.56), channel_id=1, replica_groups=mesh['rep'=2,'fs'=4,'tp'=4] {'tp'}, use_global_device_ids=true, to_apply=%region_3.4 | all-reduce | flops 1024 | bytes 8192 | tf_op jit(solution)/shard_map/psum | solution.py:90
  108.3 1.0 add_convert_fusion.1
  109.3 0.0 all-gather.9.cloned.1.call-update
  109.3 0.0 copy-start.4
  109.3 0.0 all-gather.13.cloned.1.call-start
  109.4 1.0 convert_element_type.77
  110.4 0.0 all-gather.13.cloned.1.call-update
  110.4 0.0 copy-start.11
  110.4 0.0 copy-start.12
  110.4 0.0 copy-start.10
  110.5 0.0 all-gather.17.cloned.1.call-start
  110.5 0.5 copy-done.4
  111.0 1.0 convert_element_type.79
  112.0 0.0 all-gather.17.cloned.1.call-update
  112.0 0.0 all-gather.15.cloned.1.call-start
  112.1 0.1 slice_reduce_fusion.4
  112.2 2.2 all-gather.11.cloned.1.call-done
  114.4 23.7 %all-gather.9.cloned.1.call-done = bf16[512,2048]{0,1:T(8,128)(2,1)} async-done(((bf16[512,512]{0,1:T(8,128)(2,1)}), bf16[512,2048]{0,1:T(8,128)(2,1)}) %all-gather.9.cloned.1.call-update) | async-done | bytes 2097168 | tf_op jit(solution)/shard_map/all_gather | solution.py:103
  138.2 4.4 %convolution_multiply_fusion.1 = f32[512,768]{1,0:T(8,128)S(1)} fusion(bf16[512,2048]{0,1:T(8,128)(2,1)} %all-gather.9.cloned.1.call-done, bf16[2048,768]{1,0:T(8,128)(2,1)} %all-gather.11.cloned.1.call-done, f32[768]{0:T(1024)S(1)} %get-tuple-element.18), kind=kOutput, calls=%fused_computation.17 | convolution fusion | flops 1611005952 | bytes 6818816 | tf_op jit(solution)/shard_map/dot_general | solution.py:108
  142.5 60.5 %all-gather.13.cloned.1.call-done = bf16[2048,768]{1,0:T(8,128)(2,1)} async-done(((bf16[512,768]{1,0:T(8,128)(2,1)}), bf16[2048,768]{1,0:T(8,128)(2,1)}) %all-gather.13.cloned.1.call-update) | async-done | bytes 3145744 | tf_op jit(solution)/shard_map/all_gather | solution.py:106
  203.1 4.4 %convolution_multiply_fusion = f32[512,768]{1,0:T(8,128)S(1)} fusion(bf16[512,2048]{0,1:T(8,128)(2,1)} %all-gather.9.cloned.1.call-done, bf16[2048,768]{1,0:T(8,128)(2,1)} %all-gather.13.cloned.1.call-done, f32[768]{0:T(1024)S(1)} %get-tuple-element.17), kind=kOutput, calls=%fused_computation.16 | convolution fusion | flops 1611005952 | bytes 6818816 | tf_op jit(solution)/shard_map/dot_general | solution.py:109
  207.4 0.9 fusion.2
  208.4 0.0 copy-start.1
  208.4 0.0 copy-start.16
  208.4 1.4 fusion.9
  209.8 0.0 all-gather.15.cloned.1.call-update
  209.8 0.8 dynamic_slice.14
  210.5 0.8 dynamic_slice.15
  211.3 55.3 %all-gather.17.cloned.1.call-done = bf16[3072,512]{1,0:T(8,128)(2,1)} async-done(((bf16[768,512]{1,0:T(8,128)(2,1)}), bf16[3072,512]{1,0:T(8,128)(2,1)}) %all-gather.17.cloned.1.call-update) | async-done | bytes 3145744 | tf_op jit(solution)/shard_map/all_gather | solution.py:117
  266.6 28.6 %all-gather.15.cloned.1.call-done = bf16[512,3072]{1,0:T(8,128)(2,1)} async-done(((bf16[512,768]{1,0:T(8,128)(2,1)}), bf16[512,3072]{1,0:T(8,128)(2,1)}) %all-gather.15.cloned.1.call-update) | async-done | bytes 3145744 | tf_op jit(solution)/shard_map/all_gather | solution.py:115
  295.2 4.8 %fusion.25 = (f32[512]{0:T(512)S(1)}, f32[512]{0:T(512)S(1)}, f32[512,512]{0,1:T(8,128)S(1)}) fusion(f32[512]{0:T(512)S(1)} %copy-done.16, bf16[512,3072]{1,0:T(8,128)(2,1)} %all-gather.15.cloned.1.call-done, bf16[3072,512]{1,0:T(8,128)(2,1)} %all-gather.17.cloned.1.call-done, bf16[512,512]{0,1:T(8,128)(2,1)S(1)} %copy-done.1), kind=kOutput, calls=%fused_computation.64 | convolution fusion | flops 1612446720 | bytes 7870464 | tf_op jit(solution)/shard_map/dot_general | solution.py:27
  300.0 5.9 %all-reduce.3 = (f32[512,1]{0,1:T(1,128)S(1)}, f32[512,1]{0,1:T(1,128)S(1)}) all-reduce(f32[512,1]{0,1:T(1,128)S(1)} %bitcast.59, f32[512,1]{0,1:T(1,128)S(1)} %bitcast.58), channel_id=1, replica_groups=mesh['rep'=2,'fs'=4,'tp'=4] {'tp'}, use_global_device_ids=true, to_apply=%region_7.8 | all-reduce | flops 1024 | bytes 8192 | tf_op jit(solution)/shard_map/psum | solution.py:121
  305.9 0.2 add_convert_fusion
  306.1 1.0 copy.23
  (27 shorter events, 0.2 us)
Async XLA Ops:
  6.5 83.1 %all-gather.7.cloned.1.call-start = ((), (), s32[]{:S(2)}) async-start(), calls=%async_computation | async-start | bytes 2621440 | tf_op jit(solution)/shard_map/all_gather | solution.py:68
  7.3 2.6 copy-start.2
  7.3 3.6 %copy-start.6 = (f32[512,128]{1,0:T(8,128)S(1)}, f32[512,128]{1,0:T(8,128)}, u32[]{:S(2)}) copy-start(f32[512,128]{1,0:T(8,128)} %param.22) | copy-start | bytes 786436
  7.3 107.2 %all-gather.11.cloned.1.call-start = ((), (), s32[]{:S(2)}) async-start(), calls=%async_computation.2 | async-start | bytes 3932160 | tf_op jit(solution)/shard_map/all_gather | solution.py:105
  9.8 1.1 copy-start.7
  9.8 1.2 copy-start.8
  9.8 1.2 copy-start.9
  9.8 128.4 %all-gather.9.cloned.1.call-start = ((), (), s32[]{:S(2)}) async-start(), calls=%async_computation.1 | async-start | bytes 2621440 | tf_op jit(solution)/shard_map/all_gather | solution.py:103
  11.0 78.6 %copy-start.13 = (f32[3,128]{1,0:T(4,128)S(1)}, f32[3,128]{1,0:T(4,128)}, u32[]{:S(2)}) copy-start(f32[3,128]{1,0:T(4,128)} %param.23) | copy-start | bytes 4612
  11.0 78.6 %copy-start.14 = (f32[3,128]{1,0:T(4,128)S(1)}, f32[3,128]{1,0:T(4,128)}, u32[]{:S(2)}) copy-start(f32[3,128]{1,0:T(4,128)} %param.24) | copy-start | bytes 4612
  89.6 2.5 copy-start
  92.9 7.8 %copy-start.5 = (bf16[512,512]{0,1:T(8,128)(2,1)S(1)}, bf16[512,512]{0,1:T(8,128)(2,1)}, u32[]{:S(2)}) copy-start(bf16[512,512]{0,1:T(8,128)(2,1)} %copy.22) | copy-start | bytes 1572868
  92.9 7.8 %copy-start.15 = (f32[512]{0:T(512)S(1)}, f32[512]{0:T(512)}, u32[]{:S(2)}) copy-start(f32[512]{0:T(512)} %param.26) | copy-start | bytes 6148
  101.3 8.1 %copy-start.3 = (f32[512,768]{1,0:T(8,128)S(1)}, f32[512,768]{1,0:T(8,128)}, u32[]{:S(2)}) copy-start(f32[512,768]{1,0:T(8,128)} %param.30) | copy-start | bytes 4718596
  109.3 1.7 copy-start.4
  109.3 93.8 %all-gather.13.cloned.1.call-start = ((), (), s32[]{:S(2)}) async-start(), calls=%async_computation.3 | async-start | bytes 3932160 | tf_op jit(solution)/shard_map/all_gather | solution.py:106
  110.4 1.6 copy-start.11
  110.4 1.7 copy-start.12
  110.4 1.7 copy-start.10
  110.5 156.2 %all-gather.17.cloned.1.call-start = ((), (), s32[]{:S(2)}) async-start(), calls=%async_computation.5 | async-start | bytes 3932160 | tf_op jit(solution)/shard_map/all_gather | solution.py:117
  112.0 183.2 %all-gather.15.cloned.1.call-start = ((), (), s32[]{:S(2)}) async-start(), calls=%async_computation.4 | async-start | bytes 3932160 | tf_op jit(solution)/shard_map/all_gather | solution.py:115
  208.4 86.8 %copy-start.1 = (bf16[512,512]{0,1:T(8,128)(2,1)S(1)}, bf16[512,512]{0,1:T(8,128)(2,1)}, u32[]{:S(2)}) copy-start(bf16[512,512]{0,1:T(8,128)(2,1)} %add_convert_fusion.1) | copy-start | bytes 1572868
  208.4 86.8 %copy-start.16 = (f32[512]{0:T(512)S(1)}, f32[512]{0:T(512)}, u32[]{:S(2)}) copy-start(f32[512]{0:T(512)} %param.35) | copy-start | bytes 6148
Sparse Core Ops, SparseCore 0:
  8.9 25.2 all-gather.6
  35.8 78.6 all-gather.10
  116.0 22.1 all-gather.8
  139.6 63.4 all-gather.12
  204.5 62.0 all-gather.16
  268.0 27.1 all-gather.14
where the time goes:
time: 314 us
  waiting for transfers between devices  171 us (54%)
  blocking collectives  96.9 us (31%)
  matrix products  18 us (6%)
  between operations  13.8 us (4%)
  other arithmetic  8.13 us (3%)
  local copies, waits for them, and re-layouts  5.76 us (2%)
    all_gather x1, waiting for transfers between devices, local(): lax.all_gather(lowered(gate_proj), 'fs', axis=0, tiled=True)  60.5 us
    all_gather x1, waiting for transfers between devices, local(): lax.all_gather(lowered(down_proj), 'fs', axis=0, tiled=True)  55.3 us
    all_gather x1, waiting for transfers between devices, local(): hidden_whole = lax.all_gather(hidden, 'tp', axis=1, tiled=True)  28.6 us
    all_gather x1, waiting for transfers between devices, local(): normed_whole = lax.all_gather(normed, 'tp', axis=1, tiled=True)  23.7 us
    all_gather x1, blocking collectives, local(): lax.all_gather(lowered(outer_gate), 'fs', axis=0, tiled=True)  22.6 us
    all_gather x1, blocking collectives, local(): lax.all_gather(lowered(mixer_out), 'fs', axis=0, tiled=True)  20.2 us
    all_gather x1, blocking collectives, local(): lax.all_gather(lowered(mixer_value), 'fs', axis=0, tiled=True)  17.4 us
    all_gather x1, blocking collectives, local(): lax.all_gather(lowered(inner_gate), 'fs', axis=0, tiled=True)  16.9 us
  transfers between devices with their start and end apart: 6, of which 5 were waited for; matrix products, arithmetic and copies ran while one was open for 8% of the time, Pallas kernels for 0%

commit v1 on v0

--- a/solution.py
+++ b/solution.py
@@ -100,7 +100,12 @@
         own_columns(first_gain, own_width),
         own_columns(first_shift, own_width),
     ).astype(jnp.bfloat16)
-    normed_whole = lax.all_gather(normed, "tp", axis=1, tiled=True)
+    ring = [normed]
+    for hop in range(3):
+        ring.append(lax.ppermute(ring[-1], "tp", [(dev, (dev + 1) % 4) for dev in range(4)]))
+    normed_whole = jnp.roll(
+        jnp.concatenate(ring[::-1], axis=1), (lax.axis_index("tp") + 1) * ring[0].shape[1], axis=1
+    )
     up_matrix, gate_matrix = (
         lax.all_gather(lowered(up_proj), "fs", axis=0, tiled=True),
         lax.all_gather(lowered(gate_proj), "fs", axis=0, tiled=True),

time: 314 us -> 290 us (0.924)
  waiting for transfers between devices: 171 us -> 142 us
  local copies, waits for them, and re-layouts: 5.76 us -> 9.98 us
    all_gather x1, waiting for transfers between devices: 60.5 us -> 0.01 us  [local(): lax.all_gather(lowered(gate_proj), 'fs', axis=0, tiled=True)]
    all_gather x1, waiting for transfers between devices: 2.23 us -> 31.3 us  [local(): lax.all_gather(lowered(up_proj), 'fs', axis=0, tiled=True)]
    ppermute x0 -> x3, waiting for transfers between devices: none -> 25.7 us  [local(): lax.ppermute(ring[-1], 'tp', [(dev, (dev + 1) % 4) for dev in range(4)])]
    all_gather x1 -> x0, waiting for transfers between devices: 23.7 us -> none  [local(): normed_whole = lax.all_gather(normed, 'tp', axis=1, tiled=True)]
    unnamed x35 -> x37, local copies, waits for them, and re-layouts: 1.59 us -> 5.81 us
  transfers between devices with their start and end apart: 6 -> 8, of which waited for: 5 -> 6; matrix products, arithmetic and copies ran while one was open for 8% -> 11% of each run, Pallas kernels for 0% -> 0%
where the time goes in v1:
time: 290 us
  waiting for transfers between devices  142 us (49%)
  blocking collectives  97.2 us (34%)
  matrix products  18 us (6%)
  between operations  13.4 us (5%)
  local copies, waits for them, and re-layouts  9.98 us (3%)
  other arithmetic  9.29 us (3%)
    all_gather x1, waiting for transfers between devices, local(): lax.all_gather(lowered(down_proj), 'fs', axis=0, tiled=True)  55.3 us
    all_gather x1, waiting for transfers between devices, local(): lax.all_gather(lowered(up_proj), 'fs', axis=0, tiled=True)  31.3 us
    all_gather x1, waiting for transfers between devices, local(): hidden_whole = lax.all_gather(hidden, 'tp', axis=1, tiled=True)  28.6 us
    ppermute x3, waiting for transfers between devices, local(): lax.ppermute(ring[-1], 'tp', [(dev, (dev + 1) % 4) for dev in range(4)])  25.7 us
    all_gather x1, blocking collectives, local(): lax.all_gather(lowered(outer_gate), 'fs', axis=0, tiled=True)  23.2 us
    all_gather x1, blocking collectives, local(): lax.all_gather(lowered(mixer_out), 'fs', axis=0, tiled=True)  20.1 us
    all_gather x1, blocking collectives, local(): lax.all_gather(lowered(mixer_value), 'fs', axis=0, tiled=True)  17.4 us
    all_gather x1, blocking collectives, local(): lax.all_gather(lowered(inner_gate), 'fs', axis=0, tiled=True)  16.8 us
  transfers between devices with their start and end apart: 8, of which 6 were waited for; matrix products, arithmetic and copies ran while one was open for 11% of the time, Pallas kernels for 0%

profile of v1, /device:TPU:0, one launch (start us, length us, event | category | flops | bytes accessed | tf_op | source)
XLA Modules:
  0.0 289.7 jit_solution(9243595630912566032)
XLA Ops:
  6.5 0.7 all-gather.6.cloned.1.call-update
  7.3 0.0 all-gather.10.cloned.1.call-start
  7.3 2.4 convert_element_type.77
  9.7 0.0 all-gather.10.cloned.1.call-update
  9.7 0.0 all-gather.8.cloned.1.call-start
  9.8 1.0 convert_element_type.76
  10.8 0.0 all-gather.8.cloned.1.call-update
  10.8 0.0 copy-start.11
  10.8 0.0 copy-start.4
  10.8 0.0 copy-start.5
  10.8 0.0 all-gather.14.cloned.1.call-start
  10.9 0.5 copy-done.3
  11.4 1.0 convert_element_type.79
  12.4 0.0 all-gather.14.cloned.1.call-update
  12.4 0.0 copy-start.7
  12.4 0.0 all-gather.12.cloned.1.call-start
  12.5 0.2 copy.22
  12.7 0.0 copy-done.11
  12.7 17.4 %all_gather.33 = bf16[2048,128]{1,0:T(8,128)(2,1)S(1)} all-gather(bf16[512,128]{1,0:T(8,128)(2,1)S(1)} %convert_element_type.69), channel_id=1, replica_groups=mesh['rep'=2,'fs'=4,'tp'=4] {'fs'}, dimensions={0}, use_global_device_ids=true | all-gather | bytes 655360 | tf_op jit(solution)/shard_map/all_gather | solution.py:74
  30.1 0.0 copy-done.5
  30.1 16.8 %all_gather.32 = bf16[2048,128]{1,0:T(8,128)(2,1)S(1)} all-gather(bf16[512,128]{1,0:T(8,128)(2,1)S(1)} %convert_element_type.66), channel_id=1, replica_groups=mesh['rep'=2,'fs'=4,'tp'=4] {'fs'}, dimensions={0}, use_global_device_ids=true | all-gather | bytes 655360 | tf_op jit(solution)/shard_map/all_gather | solution.py:73
  47.0 23.2 %all_gather.31 = bf16[2048,128]{1,0:T(8,128)(2,1)S(1)} all-gather(bf16[512,128]{1,0:T(8,128)(2,1)S(1)} %convert_element_type.63), channel_id=1, replica_groups=mesh['rep'=2,'fs'=4,'tp'=4] {'fs'}, dimensions={0}, use_global_device_ids=true | all-gather | bytes 655360 | tf_op jit(solution)/shard_map/all_gather | solution.py:72
  70.3 20.1 %all_gather.35 = bf16[512,512]{1,0:T(8,128)(2,1)S(1)} all-gather(bf16[128,512]{1,0:T(8,128)(2,1)S(1)} %convert_element_type.73), channel_id=1, replica_groups=mesh['rep'=2,'fs'=4,'tp'=4] {'fs'}, dimensions={0}, use_global_device_ids=true | all-gather | bytes 655360 | tf_op jit(solution)/shard_map/all_gather | solution.py:86
  90.4 0.8 dynamic_slice.16
  91.1 0.8 dynamic_slice.17
  91.9 2.5 fusion.30
  94.4 0.7 fusion.28
  95.1 0.0 copy-start.13
  95.1 0.1 fusion.33
  95.2 0.7 fusion.25
  95.9 6.8 %all_gather.34 = bf16[512,512]{1,0:T(8,128)(2,1)S(1)} all-gather(bf16[512,128]{1,0:T(8,128)(2,1)S(1)} %fusion.25), channel_id=1, replica_groups=mesh['rep'=2,'fs'=4,'tp'=4] {'tp'}, dimensions={1}, use_global_device_ids=true | all-gather | bytes 655360 | tf_op jit(solution)/shard_map/all_gather | solution.py:84
  102.7 0.6 fusion.38
  103.3 7.0 %all-reduce.4 = (f32[512,1]{0,1:T(1,128)S(1)}, f32[512,1]{0,1:T(1,128)S(1)}) all-reduce(f32[512,1]{0,1:T(1,128)S(1)} %bitcast.59, f32[512,1]{0,1:T(1,128)S(1)} %bitcast.58), channel_id=1, replica_groups=mesh['rep'=2,'fs'=4,'tp'=4] {'tp'}, use_global_device_ids=true, to_apply=%region_3.4 | all-reduce | flops 1024 | bytes 8192 | tf_op jit(solution)/shard_map/psum | solution.py:90
  110.3 0.2 add_convert_fusion.1
  110.6 0.1 collective-permute-start
  110.6 8.6 %collective-permute-done = bf16[512,512]{0,1:T(8,128)(2,1)S(1)} collective-permute-done((bf16[512,512]{0,1:T(8,128)(2,1)S(1)}, bf16[512,512]{0,1:T(8,128)(2,1)S(1)}, u32[]{:S(2)}, u32[]{:S(2)}) %collective-permute-start) | collective-permute-done | bytes 524320 | tf_op jit(solution)/shard_map/ppermute | solution.py:105
  119.2 0.0 collective-permute-start.1
  119.2 8.6 %collective-permute-done.1 = bf16[512,512]{0,1:T(8,128)(2,1)S(1)} collective-permute-done((bf16[512,512]{0,1:T(8,128)(2,1)S(1)}, bf16[512,512]{0,1:T(8,128)(2,1)S(1)}, u32[]{:S(2)}, u32[]{:S(2)}) %collective-permute-start.1) | collective-permute-done | bytes 524320 | tf_op jit(solution)/shard_map/ppermute | solution.py:105
  127.8 0.0 collective-permute-start.2
  127.9 0.1 slice_reduce_fusion.4
  128.0 8.5 %collective-permute-done.2 = bf16[512,512]{0,1:T(8,128)(2,1)S(1)} collective-permute-done((bf16[512,512]{0,1:T(8,128)(2,1)S(1)}, bf16[512,512]{0,1:T(8,128)(2,1)S(1)}, u32[]{:S(2)}, u32[]{:S(2)}) %collective-permute-start.2) | collective-permute-done | bytes 524320 | tf_op jit(solution)/shard_map/ppermute | solution.py:105
  136.4 0.8 constant_dynamic-update-slice_fusion.7
  137.2 0.8 constant_dynamic-update-slice_fusion.6
  138.1 0.9 constant_dynamic-update-slice_fusion.5
  138.9 1.0 constant_dynamic-update-slice_fusion.4
  140.0 0.8 constant_dynamic-update-slice_fusion.3
  140.8 0.8 constant_dynamic-update-slice_fusion.2
  141.6 0.8 constant_dynamic-update-slice_fusion.1
  142.5 1.0 constant_dynamic-update-slice_fusion
  143.5 4.4 %fusion.17 = f32[512,768]{1,0:T(8,128)S(1)} fusion(bf16[2048,768]{1,0:T(8,128)(2,1)} %all-gather.10.cloned.1.call-done, bf16[512,4096]{0,1:T(8,128)(2,1)} %constant_dynamic-update-slice_fusion, s32[]{:T(128)S(6)} %select_n.21, f32[768]{0:T(1024)S(1)} %get-tuple-element.17), kind=kOutput, calls=%fused_computation.21 | convolution fusion | flops 1611005952 | bytes 6818820 | tf_op jit(solution)/shard_map/dot_general | solution.py:114
  147.9 31.3 %all-gather.8.cloned.1.call-done = bf16[2048,768]{1,0:T(8,128)(2,1)} async-done(((bf16[512,768]{1,0:T(8,128)(2,1)}), bf16[2048,768]{1,0:T(8,128)(2,1)}) %all-gather.8.cloned.1.call-update) | async-done | bytes 3145744 | tf_op jit(solution)/shard_map/all_gather | solution.py:110
  179.1 4.4 %fusion.14 = f32[512,768]{1,0:T(8,128)S(1)} fusion(bf16[2048,768]{1,0:T(8,128)(2,1)} %all-gather.8.cloned.1.call-done, bf16[512,4096]{0,1:T(8,128)(2,1)} %constant_dynamic-update-slice_fusion, s32[]{:T(128)S(6)} %select_n.21, f32[768]{0:T(1024)S(1)} %get-tuple-element.18), kind=kOutput, calls=%fused_computation.20 | convolution fusion | flops 1611005952 | bytes 6818820 | tf_op jit(solution)/shard_map/dot_general | solution.py:113
  183.5 0.9 fusion.6
  184.4 0.0 copy-start.14
  184.4 1.3 fusion.13
  185.8 0.0 all-gather.12.cloned.1.call-update
  185.8 0.8 dynamic_slice.19
  186.6 0.8 dynamic_slice.20
  187.4 55.3 %all-gather.14.cloned.1.call-done = bf16[3072,512]{1,0:T(8,128)(2,1)} async-done(((bf16[768,512]{1,0:T(8,128)(2,1)}), bf16[3072,512]{1,0:T(8,128)(2,1)}) %all-gather.14.cloned.1.call-update) | async-done | bytes 3145744 | tf_op jit(solution)/shard_map/all_gather | solution.py:122
  242.7 28.6 %all-gather.12.cloned.1.call-done = bf16[512,3072]{1,0:T(8,128)(2,1)} async-done(((bf16[512,768]{1,0:T(8,128)(2,1)}), bf16[512,3072]{1,0:T(8,128)(2,1)}) %all-gather.12.cloned.1.call-update) | async-done | bytes 3145744 | tf_op jit(solution)/shard_map/all_gather | solution.py:120
  271.3 4.8 %fusion.37 = (f32[512]{0:T(512)S(1)}, f32[512]{0:T(512)S(1)}, f32[512,512]{0,1:T(8,128)S(1)}) fusion(f32[512]{0:T(512)S(1)} %copy-done.14, bf16[512,3072]{1,0:T(8,128)(2,1)} %all-gather.12.cloned.1.call-done, bf16[3072,512]{1,0:T(8,128)(2,1)} %all-gather.14.cloned.1.call-done, bf16[512,512]{0,1:T(8,128)(2,1)S(1)} %add_convert_fusion.1), kind=kOutput, calls=%fused_computation.78 | convolution fusion | flops 1612446720 | bytes 7870464 | tf_op jit(solution)/shard_map/dot_general | solution.py:27
  276.1 5.9 %all-reduce.3 = (f32[512,1]{0,1:T(1,128)S(1)}, f32[512,1]{0,1:T(1,128)S(1)}) all-reduce(f32[512,1]{0,1:T(1,128)S(1)} %bitcast.61, f32[512,1]{0,1:T(1,128)S(1)} %bitcast.60), channel_id=1, replica_groups=mesh['rep'=2,'fs'=4,'tp'=4] {'tp'}, use_global_device_ids=true, to_apply=%region_7.8 | all-reduce | flops 1024 | bytes 8192 | tf_op jit(solution)/shard_map/psum | solution.py:126
  282.0 0.2 add_convert_fusion
  282.2 1.0 copy.23
  (34 shorter events, 0.2 us)
Async XLA Ops:
  6.5 3.2 %copy-start.2 = (f32[512,768]{1,0:T(8,128)S(1)}, f32[512,768]{1,0:T(8,128)}, u32[]{:S(2)}) copy-start(f32[512,768]{1,0:T(8,128)} %param.29) | copy-start | bytes 4718596
  6.5 85.4 %all-gather.6.cloned.1.call-start = ((), (), s32[]{:S(2)}) async-start(), calls=%async_computation | async-start | bytes 2621440 | tf_op jit(solution)/shard_map/all_gather | solution.py:68
  7.3 136.2 %all-gather.10.cloned.1.call-start = ((), (), s32[]{:S(2)}) async-start(), calls=%async_computation.2 | async-start | bytes 3932160 | tf_op jit(solution)/shard_map/all_gather | solution.py:111
  9.7 1.7 copy-start.3
  9.7 169.4 %all-gather.8.cloned.1.call-start = ((), (), s32[]{:S(2)}) async-start(), calls=%async_computation.1 | async-start | bytes 3932160 | tf_op jit(solution)/shard_map/all_gather | solution.py:110
  10.8 1.7 copy-start.1
  10.8 1.9 copy-start.11
  10.8 1.9 copy-start.4
  10.8 19.3 %copy-start.5 = (f32[512,128]{1,0:T(8,128)S(1)}, f32[512,128]{1,0:T(8,128)}, u32[]{:S(2)}) copy-start(f32[512,128]{1,0:T(8,128)} %param.21) | copy-start | bytes 786436
  10.8 231.9 %all-gather.14.cloned.1.call-start = ((), (), s32[]{:S(2)}) async-start(), calls=%async_computation.4 | async-start | bytes 3932160 | tf_op jit(solution)/shard_map/all_gather | solution.py:122
  12.4 34.6 %copy-start.12 = (f32[3,128]{1,0:T(4,128)S(1)}, f32[3,128]{1,0:T(4,128)}, u32[]{:S(2)}) copy-start(f32[3,128]{1,0:T(4,128)} %param.24) | copy-start | bytes 4612
  12.4 34.6 %copy-start.6 = (f32[512,128]{1,0:T(8,128)S(1)}, f32[512,128]{1,0:T(8,128)}, u32[]{:S(2)}) copy-start(f32[512,128]{1,0:T(8,128)} %param.20) | copy-start | bytes 786436
  12.4 57.9 %copy-start.7 = (f32[128,512]{1,0:T(8,128)S(1)}, f32[128,512]{1,0:T(8,128)}, u32[]{:S(2)}) copy-start(f32[128,512]{1,0:T(8,128)} %param.25) | copy-start | bytes 786436
  12.4 258.9 %all-gather.12.cloned.1.call-start = ((), (), s32[]{:S(2)}) async-start(), calls=%async_computation.3 | async-start | bytes 3932160 | tf_op jit(solution)/shard_map/all_gather | solution.py:120
  91.9 2.5 copy-start
  95.1 7.6 %copy-start.13 = (f32[512]{0:T(512)S(1)}, f32[512]{0:T(512)}, u32[]{:S(2)}) copy-start(f32[512]{0:T(512)} %param.26) | copy-start | bytes 6148
  102.7 25.1 %copy-start.9 = (f32[2,768]{1,0:T(2,128)S(1)}, f32[2,768]{1,0:T(2,128)}, u32[]{:S(2)}) copy-start(f32[2,768]{1,0:T(2,128)} %param.31) | copy-start | bytes 18436
  102.7 25.2 %copy-start.10 = (f32[2,768]{1,0:T(2,128)S(1)}, f32[2,768]{1,0:T(2,128)}, u32[]{:S(2)}) copy-start(f32[2,768]{1,0:T(2,128)} %param.33) | copy-start | bytes 18436
  102.7 25.2 %copy-start.8 = (f32[3,2,768]{2,1,0:T(2,128)S(1)}, f32[3,2,768]{2,1,0:T(2,128)}, u32[]{:S(2)}) copy-start(f32[3,2,768]{2,1,0:T(2,128)} %param.32) | copy-start | bytes 55300
  110.6 8.7 %collective-permute-start = (bf16[512,512]{0,1:T(8,128)(2,1)S(1)}, bf16[512,512]{0,1:T(8,128)(2,1)S(1)}, u32[]{:S(2)}, u32[]{:S(2)}) collective-permute-start(bf16[512,512]{0,1:T(8,128)(2,1)S(1)} %add_convert_fusion.1), channel_id=1, source_target_pairs={{0,1},{1,2},{2,3},{3,0},{4,5},{5,6},{6,7},{7,4},{8,9},{9,10},{10,1... | collective-permute-start | bytes 1572872 | tf_op jit(solution)/shard_map/ppermute | solution.py:105
  119.2 8.6 %collective-permute-start.1 = (bf16[512,512]{0,1:T(8,128)(2,1)S(1)}, bf16[512,512]{0,1:T(8,128)(2,1)S(1)}, u32[]{:S(2)}, u32[]{:S(2)}) collective-permute-start(bf16[512,512]{0,1:T(8,128)(2,1)S(1)} %collective-permute-done), channel_id=1, source_target_pairs={{0,1},{1,2},{2,3},{3,0},{4,5},{5,6},{6,7},{7,4},{8,9},{9,10},{10,1... | collective-permute-start | bytes 1572872 | tf_op jit(solution)/shard_map/ppermute | solution.py:105
  127.8 8.6 %collective-permute-start.2 = (bf16[512,512]{0,1:T(8,128)(2,1)S(1)}, bf16[512,512]{0,1:T(8,128)(2,1)S(1)}, u32[]{:S(2)}, u32[]{:S(2)}) collective-permute-start(bf16[512,512]{0,1:T(8,128)(2,1)S(1)} %collective-permute-done.1), channel_id=1, source_target_pairs={{0,1},{1,2},{2,3},{3,0},{4,5},{5,6},{6,7},{7,4},{8,9},{9,10},{10,1... | collective-permute-start | bytes 1572872 | tf_op jit(solution)/shard_map/ppermute | solution.py:105
  184.4 86.8 %copy-start.14 = (f32[512]{0:T(512)S(1)}, f32[512]{0:T(512)}, u32[]{:S(2)}) copy-start(f32[512]{0:T(512)} %param.35) | copy-start | bytes 6148
Sparse Core Ops, SparseCore 0:
  8.9 25.2 all-gather.5
  35.8 78.5 all-gather.9
  116.0 63.1 all-gather.7
  180.6 62.0 all-gather.13
  244.1 27.1 all-gather.11
